TPU v7x, 32 devices: a whole 2x2x4 slice. The times are simulated.
32 devices in a mesh: sp: 8 (over z, y), tp: 4 (over x, core).
Axes of the slice: x: 2, y: 2, z: 4, core: 2. Of those that a mesh axis runs over, the one named last changes fastest.
Arguments:
- tokens: bfloat16 [1536, 2048], P('sp'), may hold values from -6 to 6
- norm_gain: float32 [2048], replicated, may hold values from 0.1 to 1.9
- conv_value_w: bfloat16 [2048, 1024], P('sp', 'tp'), may hold values from -0.125 to 0.125
- conv_gate_w: bfloat16 [2048, 1024], P('sp', 'tp'), may hold values from -0.125 to 0.125
- query_w: bfloat16 [2048, 1024], P('sp', 'tp'), may hold values from -0.125 to 0.125
- key_w: bfloat16 [2048, 1024], P('sp', 'tp'), may hold values from -0.125 to 0.125
- value_w: bfloat16 [2048, 1024], P('sp', 'tp'), may hold values from -0.125 to 0.125
- out_gate_w: bfloat16 [2048, 1024], P('sp', 'tp'), may hold values from -0.125 to 0.125
- conv_out_w: bfloat16 [2048, 1024], P('sp', 'tp'), may hold values from -0.125 to 0.125
- ret_out_w: bfloat16 [2048, 1024], P('sp', 'tp'), may hold values from -0.125 to 0.125
- conv_taps: bfloat16 [31, 1024], replicated, may hold values from -3 to 3
- conv_gain: float32 [1024], replicated, may hold values from 0.1 to 1.9
- ret_gain: float32 [1024], replicated, may hold values from 0.1 to 1.9
- log_decay: float32 [8, 1536], P('tp', 'sp'), may hold values from -1 to 0, as said below
Outputs:
- mixed: bfloat16 [1536, 2048], P(('sp', 'tp'))
Inputs may be any that keep to these rules, and one draw needn't show every extreme that they name: `log_decay`: every entry is at most zero.
All inputs are finite; a program needn't handle non-finite values.
Results may differ from a plain program's by a relative error of at most 0.03.
Values may be sent and summed in bfloat16 or wider, within the bound.
A program may use at most 64 MiB of HBM per device.

v0:
```python
import jax
import jax.numpy as jnp
from jax import lax
from jax.sharding import PartitionSpec as P

CONV_DIM = 1024
HEAD_DIM = 128
CONV_WIDTH = 31


EPSILON = 1e-06
ROPE_BASE = 10000.0


def from_behind(value, axis, steps):
    count = lax.axis_size(axis)
    first, last = (max(0, -steps), min(count, count - steps))
    return lax.ppermute(value, axis, [(source, source + steps) for source in range(first, last)])


def carried_in(x, axis, combine, identity):
    peers, here = (lax.axis_size(axis), lax.axis_index(axis))
    everything = jax.tree.map(
        lambda part, kind: lax.all_gather(part.astype(kind), axis), x, (jnp.bfloat16, jnp.bfloat16)
    )
    start = jax.tree.map(
        lambda part, zero: jnp.broadcast_to(jnp.asarray(zero, part.dtype), part.shape), x, identity
    )

    def turn(k, before):
        reached = k < here
        new = combine(
            before, jax.tree.map(lambda part, own: part[k].astype(own.dtype), everything, x)
        )
        return jax.tree.map(lambda a, b: jnp.where(reached, a, b), new, before)

    return lax.fori_loop(0, peers, turn, start)


def rotate(values, token_positions):
    half_dim = values.shape[-1] // 2
    frequency = ROPE_BASE ** (-jnp.arange(0, 2 * half_dim, 2, dtype=jnp.float32) / (2 * half_dim))
    angles = token_positions.astype(jnp.float32)[:, None] * frequency[None, :]
    cosine = jnp.cos(angles)[:, None, :]
    sine_part = jnp.sin(angles)[:, None, :]
    first_half = values[..., :half_dim]
    second = values[..., half_dim:]
    return jnp.concatenate(
        [first_half * cosine - second * sine_part, first_half * sine_part + second * cosine],
        axis=-1,
    )


def combine_state(earlier, later):
    return (earlier[0] * later[0], later[1] + later[0][:, None, None] * earlier[1])


def project(normed, weight):
    return jnp.dot(normed, weight, preferred_element_type=jnp.float32).astype(jnp.bfloat16)


def per_device(
    tokens,
    norm_gain,
    conv_value_w,
    conv_gate_w,
    query_w,
    key_w,
    value_w,
    out_gate_w,
    conv_out_w,
    ret_out_w,
    conv_taps,
    conv_gain,
    ret_gain,
    log_decay,
):
    row_count = tokens.shape[0]
    conv_cols = conv_value_w.shape[1]
    ret_cols = query_w.shape[1]
    head_count = ret_cols // HEAD_DIM
    tp_index = lax.axis_index("tp")
    seq_index = lax.axis_index("sp")
    tok_float = tokens.astype(jnp.float32)
    normed = (
        tok_float
        * lax.rsqrt(jnp.mean(tok_float * tok_float, axis=-1, keepdims=True) + EPSILON)
        * norm_gain
    ).astype(jnp.bfloat16)
    gathered = (
        lax.all_gather(conv_value_w, "sp", axis=0, tiled=True),
        lax.all_gather(conv_gate_w, "sp", axis=0, tiled=True),
        lax.all_gather(conv_out_w, "sp", axis=0, tiled=True),
        lax.all_gather(query_w, "sp", axis=0, tiled=True),
        lax.all_gather(key_w, "sp", axis=0, tiled=True),
        lax.all_gather(value_w, "sp", axis=0, tiled=True),
        lax.all_gather(out_gate_w, "sp", axis=0, tiled=True),
        lax.all_gather(ret_out_w, "sp", axis=0, tiled=True),
    )
    conv_set = gathered[:3]
    ret_set = gathered[3:]
    conv_gated = (
        project(normed, conv_set[0]).astype(jnp.float32)
        * jax.nn.sigmoid(project(normed, conv_set[1]).astype(jnp.float32))
    ).astype(jnp.bfloat16)
    edge_rows = conv_gated[row_count - CONV_WIDTH + 1 :]
    before = from_behind(edge_rows, "sp", 1)
    token_positions = seq_index * row_count + jnp.arange(row_count, dtype=jnp.int32)
    query_rows = (
        rotate(
            project(normed, ret_set[0])
            .astype(jnp.float32)
            .reshape(row_count, head_count, HEAD_DIM),
            token_positions,
        )
        * HEAD_DIM ** (-0.5)
    ).astype(jnp.bfloat16)
    key_rows = rotate(
        project(normed, ret_set[1]).astype(jnp.float32).reshape(row_count, head_count, HEAD_DIM),
        token_positions,
    ).astype(jnp.bfloat16)
    value_rows = project(normed, ret_set[2]).reshape(row_count, head_count, HEAD_DIM)
    out_gate = project(normed, ret_set[3])
    running = jnp.cumsum(log_decay, axis=1)
    to_end = jnp.exp(running[:, -1:] - running)
    key_weighted = (key_rows.astype(jnp.float32) * jnp.transpose(to_end)[:, :, None]).astype(
        jnp.bfloat16
    )
    block_state = jnp.einsum(
        "thd,the->hde", key_weighted, value_rows, preferred_element_type=jnp.float32
    )
    decay_total = jnp.exp(running[:, -1])
    unit_decay = jnp.ones_like(decay_total)
    empty_state = jnp.zeros_like(block_state)
    carried = carried_in((decay_total, block_state), "sp", combine_state, (unit_decay, empty_state))
    prior_state = carried[1]
    taps_local = lax.dynamic_slice_in_dim(conv_taps, tp_index * conv_cols, conv_cols, 1).astype(
        jnp.float32
    )
    conv_gain_local = lax.dynamic_slice_in_dim(conv_gain, tp_index * conv_cols, conv_cols, 0)
    padded = jnp.concatenate([before, conv_gated], axis=0)
    conv_sum = jnp.zeros((row_count, conv_cols), jnp.float32)
    for tap_index in range(CONV_WIDTH):
        conv_sum = (
            conv_sum
            + padded[tap_index : tap_index + row_count].astype(jnp.float32) * taps_local[tap_index]
        )
    stat_sums = lax.psum((jnp.sum(conv_sum, axis=-1), jnp.sum(conv_sum * conv_sum, axis=-1)), "tp")
    chan_mean = stat_sums[0][:, None] / CONV_DIM
    chan_var = stat_sums[1][:, None] / CONV_DIM - chan_mean * chan_mean
    conv_hidden = jax.nn.silu(
        (conv_sum - chan_mean) * lax.rsqrt(chan_var + EPSILON) * conv_gain_local
    ).astype(jnp.bfloat16)
    token_iota = jnp.arange(row_count, dtype=jnp.int32)
    later_mask = token_iota[:, None] >= token_iota[None, :]
    log_gap = running[:, :, None] - running[:, None, :]
    decay_matrix = jnp.where(
        later_mask[None], jnp.exp(jnp.where(later_mask[None], log_gap, 0.0)), 0.0
    )
    scores = jnp.einsum("thd,shd->hts", query_rows, key_rows, preferred_element_type=jnp.float32)
    weights_intra = (scores * decay_matrix).astype(jnp.bfloat16)
    intra_part = jnp.einsum(
        "hts,shd->thd", weights_intra, value_rows, preferred_element_type=jnp.float32
    )
    cross_part = (
        jnp.einsum(
            "thd,hde->the",
            query_rows.astype(jnp.float32),
            prior_state,
            precision=lax.Precision.HIGHEST,
        )
        * jnp.transpose(jnp.exp(running))[:, :, None]
    )
    merged = intra_part + cross_part
    head_mean = jnp.mean(merged, axis=-1, keepdims=True)
    head_var = jnp.mean(jnp.square(merged - head_mean), axis=-1, keepdims=True)
    ret_gain_local = lax.dynamic_slice_in_dim(ret_gain, tp_index * ret_cols, ret_cols, 0)
    ret_norm = ((merged - head_mean) * lax.rsqrt(head_var + EPSILON)).reshape(
        row_count, ret_cols
    ) * ret_gain_local
    ret_hidden = (jax.nn.silu(out_gate.astype(jnp.float32)) * ret_norm).astype(jnp.bfloat16)
    contraction = (((1,), (1,)), ((), ()))
    conv_term = lax.dot_general(
        conv_hidden, conv_set[2], contraction, preferred_element_type=jnp.float32
    )
    ret_term = lax.dot_general(
        ret_hidden, ret_set[4], contraction, preferred_element_type=jnp.float32
    )
    return lax.psum_scatter(
        (conv_term + ret_term).astype(jnp.bfloat16), "tp", scatter_dimension=0, tiled=True
    )


def solution(mesh):
    return jax.shard_map(
        per_device,
        mesh=mesh,
        in_specs=(
            P("sp", None),
            P(),
            P("sp", "tp"),
            P("sp", "tp"),
            P("sp", "tp"),
            P("sp", "tp"),
            P("sp", "tp"),
            P("sp", "tp"),
            P("sp", "tp"),
            P("sp", "tp"),
            P(),
            P(),
            P(),
            P("tp", "sp"),
        ),
        out_specs=P(("sp", "tp"), None),
        check_vma=False,
    )
```

profile of v0, /device:TPU:25, one launch (start us, length us, event | category | flops | bytes accessed | tf_op | source)
XLA Modules:
  0.0 372.2 jit_solution(1183424186902870809)
XLA Ops:
  6.6 0.7 all-gather.21.cloned.1.call-update
  7.3 0.7 all-gather.23.cloned.1.call-update
  8.1 0.7 all-gather.19.cloned.1.call-update
  8.8 0.5 all-gather.11.cloned.1.call-update
  9.4 0.5 all-gather.13.cloned.1.call-update
  10.0 0.5 all-gather.15.cloned.1.call-update
  10.5 0.7 all-gather.17.cloned.1.call-update
  11.3 0.7 all-gather.25.cloned.1.call-update
  12.1 0.7 dynamic-slice_convert_fusion
  12.9 0.2 fusion.2
  13.2 0.6 reduce-window.6
  13.8 0.2 slice_reduce_fusion
  14.0 0.2 reduce-window.9
  14.5 0.6 dynamic-slice
  15.7 0.2 dynamic-update-slice
  16.0 14.0 %all-reduce.1 = bf16[16]{0:T(256)(128)(2,1)S(1)} all-reduce(bf16[16]{0:T(256)(128)(2,1)S(1)} %dynamic-update-slice), channel_id=3, replica_groups=mesh['sp'=8,'tp'=4] {'sp'}, use_global_device_ids=true, to_apply=%add.1 | all-reduce | flops 16 | bytes 64
  30.0 0.8 dynamic_slice.24
  30.8 0.8 dynamic_slice.25
  31.6 0.4 multiply_cosine_fusion
  32.0 15.5 %all-gather.21.cloned.1.call-done = bf16[2048,256]{1,0:T(8,128)(2,1)} async-done(((bf16[256,256]{1,0:T(8,128)(2,1)}), bf16[2048,256]{1,0:T(8,128)(2,1)}) %all-gather.21.cloned.1.call-update) | async-done | bytes 1048592 | tf_op jit(solution)/shard_map/all_gather | solution.py:94
  47.5 1.6 fusion.11
  49.2 39.4 %all-gather.23.cloned.1.call-done = bf16[2048,256]{1,0:T(8,128)(2,1)} async-done(((bf16[256,256]{1,0:T(8,128)(2,1)}), bf16[2048,256]{1,0:T(8,128)(2,1)}) %all-gather.23.cloned.1.call-update) | async-done | bytes 1048592 | tf_op jit(solution)/shard_map/all_gather | solution.py:95
  88.6 1.6 fusion.10
  90.4 0.5 fusion.88
  90.9 0.1 multiply_subtract_fusion
  91.0 38.8 %all-gather.19.cloned.1.call-done = bf16[2048,256]{1,0:T(8,128)(2,1)} async-done(((bf16[256,256]{1,0:T(8,128)(2,1)}), bf16[2048,256]{1,0:T(8,128)(2,1)}) %all-gather.19.cloned.1.call-update) | async-done | bytes 1048592 | tf_op jit(solution)/shard_map/all_gather | solution.py:96
  129.8 1.6 fusion.21
  131.4 0.3 convolution_convert_fusion.6
  131.8 24.8 %all-gather = bf16[16,128,128]{2,1,0:T(8,128)(2,1)S(1)} all-gather(bf16[2,128,128]{2,1,0:T(8,128)(2,1)S(1)} %convolution_convert_fusion.6), channel_id=2, replica_groups=mesh['sp'=8,'tp'=4] {'sp'}, dimensions={0}, use_global_device_ids=true | all-gather | bytes 589824 | tf_op jit(solution)/shard_map/all_gather | solution.py:24
  156.5 1.0 while.14
  157.5 14.8 %all-gather.11.cloned.1.call-done = bf16[2048,256]{1,0:T(8,128)(2,1)} async-done(((bf16[256,256]{1,0:T(8,128)(2,1)}), bf16[2048,256]{1,0:T(8,128)(2,1)}) %all-gather.11.cloned.1.call-update) | async-done | bytes 1048592 | tf_op jit(solution)/shard_map/all_gather | solution.py:91
  172.3 1.6 fusion.19
  174.0 39.5 %all-gather.13.cloned.1.call-done = bf16[2048,256]{1,0:T(8,128)(2,1)} async-done(((bf16[256,256]{1,0:T(8,128)(2,1)}), bf16[2048,256]{1,0:T(8,128)(2,1)}) %all-gather.13.cloned.1.call-update) | async-done | bytes 1048592 | tf_op jit(solution)/shard_map/all_gather | solution.py:92
  213.5 1.7 fusion.20
  215.2 2.4 collective-permute-start
  217.5 0.1 fusion.28
  217.7 0.2 fusion.9
  217.9 0.6 fusion.93
  218.5 0.3 multiply_reduce_fusion
  218.8 1.8 collective-permute-done
  220.6 0.9 fusion.87
  221.5 8.9 %all-reduce.2 = (f32[192]{0:T(256)S(1)}, f32[192]{0:T(256)S(1)}) all-reduce(f32[192]{0:T(256)S(1)} %get-tuple-element.119, f32[192]{0:T(256)S(1)} %get-tuple-element.118), channel_id=1, replica_groups=mesh['sp'=8,'tp'=4] {'tp'}, use_global_device_ids=true, to_apply=%region_4.5 | all-reduce | flops 384 | bytes 3072 | tf_op jit(solution)/shard_map/psum | solution.py:148
  230.4 24.1 %all-gather.15.cloned.1.call-done = bf16[2048,256]{1,0:T(8,128)(2,1)} async-done(((bf16[256,256]{1,0:T(8,128)(2,1)}), bf16[2048,256]{1,0:T(8,128)(2,1)}) %all-gather.15.cloned.1.call-update) | async-done | bytes 1048592 | tf_op jit(solution)/shard_map/all_gather | solution.py:93
  254.5 1.7 fusion.33
  256.2 39.4 %all-gather.17.cloned.1.call-done = bf16[2048,256]{1,0:T(8,128)(2,1)} async-done(((bf16[256,256]{1,0:T(8,128)(2,1)}), bf16[2048,256]{1,0:T(8,128)(2,1)}) %all-gather.17.cloned.1.call-update) | async-done | bytes 1048592 | tf_op jit(solution)/shard_map/all_gather | solution.py:97
  295.6 41.1 %all-gather.25.cloned.1.call-done = bf16[2048,256]{1,0:T(8,128)(2,1)} async-done(((bf16[256,256]{1,0:T(8,128)(2,1)}), bf16[2048,256]{1,0:T(8,128)(2,1)}) %all-gather.25.cloned.1.call-update) | async-done | bytes 1048592 | tf_op jit(solution)/shard_map/all_gather | solution.py:98
  336.8 3.6 fusion.1
  340.4 25.3 %reduce-scatter.2.cloned.1.call-done = bf16[48,2048]{1,0:T(8,128)(2,1)} async-done(((bf16[192,2048]{1,0:T(8,128)(2,1)}), bf16[48,2048]{1,0:T(8,128)(2,1)}) %reduce-scatter.2.cloned.1.call-update) | async-done | bytes 196624 | tf_op jit(solution)/shard_map/reduce_scatter | solution.py:189
  (57 shorter events, 1.9 us)
Async XLA Ops:
  6.5 7.9 %copy-start.3 = (u32[32]{0:T(128)S(1)}, u32[32]{0:T(128)}, u32[]{:S(2)}) copy-start(u32[32]{0:T(128)} %constant.77) | copy-start | bytes 388
  6.5 6.3 %copy-start = (bf16[192,2048]{1,0:T(8,128)(2,1)S(1)}, bf16[192,2048]{1,0:T(8,128)(2,1)}, u32[]{:S(2)}) copy-start(bf16[192,2048]{1,0:T(8,128)(2,1)} %param.16) | copy-start | bytes 2359300
  6.5 6.6 %copy-start.2 = (f32[2,192]{1,0:T(2,128)S(1)}, f32[2,192]{1,0:T(2,128)}, u32[]{:S(2)}) copy-start(f32[2,192]{1,0:T(2,128)} %param.29) | copy-start | bytes 4612
  6.5 40.9 %copy-start.1 = (f32[2048]{0:T(1024)S(1)}, f32[2048]{0:T(1024)}, u32[]{:S(2)}) copy-start(f32[2048]{0:T(1024)} %param.17) | copy-start | bytes 24580
  6.5 40.9 %all-gather.21.cloned.1.call-start = ((), (), s32[]{:S(2)}) async-start(), calls=%async_computation.6 | async-start | bytes 1179648 | tf_op jit(solution)/shard_map/all_gather | solution.py:94
  7.3 81.4 %all-gather.23.cloned.1.call-start = ((), (), s32[]{:S(2)}) async-start(), calls=%async_computation.7 | async-start | bytes 1179648 | tf_op jit(solution)/shard_map/all_gather | solution.py:95
  8.0 121.8 %all-gather.19.cloned.1.call-start = ((), (), s32[]{:S(2)}) async-start(), calls=%async_computation.5 | async-start | bytes 1179648 | tf_op jit(solution)/shard_map/all_gather | solution.py:96
  8.8 163.6 %all-gather.11.cloned.1.call-start = ((), (), s32[]{:S(2)}) async-start(), calls=%async_computation.1 | async-start | bytes 1179648 | tf_op jit(solution)/shard_map/all_gather | solution.py:91
  9.3 204.2 %all-gather.13.cloned.1.call-start = ((), (), s32[]{:S(2)}) async-start(), calls=%async_computation.2 | async-start | bytes 1179648 | tf_op jit(solution)/shard_map/all_gather | solution.py:92
  9.9 244.6 %all-gather.15.cloned.1.call-start = ((), (), s32[]{:S(2)}) async-start(), calls=%async_computation.3 | async-start | bytes 1179648 | tf_op jit(solution)/shard_map/all_gather | solution.py:93
  10.5 285.1 %all-gather.17.cloned.1.call-start = ((), (), s32[]{:S(2)}) async-start(), calls=%async_computation.4 | async-start | bytes 1179648 | tf_op jit(solution)/shard_map/all_gather | solution.py:97
  11.2 325.5 %all-gather.25.cloned.1.call-start = ((), (), s32[]{:S(2)}) async-start(), calls=%async_computation.8 | async-start | bytes 1179648 | tf_op jit(solution)/shard_map/all_gather | solution.py:98
  12.0 353.7 %reduce-scatter.2.cloned.1.call-start = ((), (), s32[]{:S(2)}) async-start(), calls=%async_computation.9 | async-start | bytes 983040 | tf_op jit(solution)/shard_map/reduce_scatter | solution.py:189
  215.2 5.4 %collective-permute-start = (bf16[30,256]{1,0:T(8,128)(2,1)S(1)}, bf16[30,256]{1,0:T(8,128)(2,1)S(1)}, u32[]{:S(2)}, u32[]{:S(2)}) collective-permute-start(bf16[30,256]{1,0:T(8,128)(2,1)S(1)} %slice.282), channel_id=1, source_target_pairs={{0,4},{4,8},{8,12},{12,16},{16,20},{20,24},{24,28},{1,5},{5,9},{9,... | collective-permute-start | bytes 46088 | tf_op jit(solution)/shard_map/ppermute | solution.py:18
Sparse Core Ops, SparseCore 0:
  9.5 37.9 all-gather.20
  49.6 39.0 all-gather.22
  90.8 38.9 all-gather.18
  131.8 40.5 all-gather.10
  174.3 39.1 all-gather.12
  215.5 38.9 all-gather.14
  256.6 38.9 all-gather.16
  297.8 38.9 all-gather.24
  340.5 25.0 reduce-scatter.1
where the time goes:
time: 375 us; the launch traced here: 372 us
  waiting for transfers between devices  285 us (76%)
  blocking collectives  47.6 us (13%)
  matrix products  14.7 us (4%)
  between operations  14.1 us (4%)
  other arithmetic  4.59 us (1%)
    all_gather x1, waiting for transfers between devices, per_device(): lax.all_gather(ret_out_w, 'sp', axis=0, tiled=True)  41.1 us
    all_gather x1, waiting for transfers between devices, per_device(): lax.all_gather(conv_gate_w, 'sp', axis=0, tiled=True)  39.5 us
    all_gather x1, waiting for transfers between devices, per_device(): lax.all_gather(key_w, 'sp', axis=0, tiled=True)  39.4 us
    all_gather x1, waiting for transfers between devices, per_device(): lax.all_gather(out_gate_w, 'sp', axis=0, tiled=True)  39.4 us
    all_gather x1, waiting for transfers between devices, per_device(): lax.all_gather(value_w, 'sp', axis=0, tiled=True)  38.8 us
    reduce_scatter x1, waiting for transfers between devices, per_device(): lax.psum_scatter((conv_term + ret_term).astype(jnp.bfloat16), 'tp', scatt...  25.3 us
    all_gather x1, blocking collectives, carried_in(): lax.all_gather(part.astype(kind), axis)  24.8 us
    all_gather x1, waiting for transfers between devices, per_device(): lax.all_gather(conv_out_w, 'sp', axis=0, tiled=True)  24.1 us
  transfers between devices with their start and end apart: 10, of which 10 were waited for; matrix products, arithmetic and copies ran while one was open for 5% of the time, Pallas kernels for 0%

commit v1 on v0

v1 whole, which is shorter than its diff:
```python
import functools

import jax
import jax.numpy as jnp
import numpy as np
from jax import lax
from jax.experimental import pallas as pl
from jax.experimental.pallas import tpu as pltpu
from jax.sharding import PartitionSpec as P

HEAD_DIM = 128
EPSILON = 1e-06
ROPE_BASE = 10000.0
F32 = jnp.float32
BF16 = jnp.bfloat16
N_PROJ = 6
HALO = 32
CHUNKS = 4


def dot(a, b, ca=1, cb=0):
    return lax.dot_general(a, b, (((ca,), (cb,)), ((), ())), preferred_element_type=F32)


def kernel(
    n_s,
    n_t,
    conv_dim,
    tok_ref,
    gain_ref,
    kw_ref,
    vw_ref,
    cvw_ref,
    cgw_ref,
    qw_ref,
    ogw_ref,
    cow_ref,
    row_ref,
    taps_ref,
    cgain_ref,
    rgain_ref,
    ld_ref,
    cj_ref,
    sj_ref,
    cb_ref,
    sb_ref,
    out_ref,
    tok,
    x_self,
    x_send,
    x_recv,
    wbuf,
    obuf,
    acc,
    p_send,
    p_recv,
    decay,
    run_cols,
    tot_send,
    tot_buf,
    st_send,
    st_buf,
    state,
    halo_send,
    halo_recv,
    xp,
    csum,
    stat_send,
    stat_buf,
    hid,
    r_send,
    r_buf,
    qkv,
    loc_sem,
    x_sem,
    ws_sem,
    wr_sem,
    os_sem,
    or_sem,
    oy_sem,
    p_sem,
    ts_sem,
    tr_sem,
    ss_sem,
    sr_sem,
    h_sem,
    stat_sem,
    rs_sem,
):
    rows = tok.shape[0]
    wrows, cols = kw_ref.shape
    heads = cols // HEAD_DIM
    k = max(1, 128 // wrows)
    n_o = n_s // 2
    me = lax.axis_index("sp")
    mt = lax.axis_index("tp")
    half = lax.rem(me // k, 2)
    idx = (me // (2 * k)) * k + lax.rem(me, k)
    pair = me + k * (1 - 2 * half)

    def member(i):
        return (i // k) * (2 * k) + half * k + lax.rem(i, k)

    def remote(src, dst, ssem, rsem, where):
        return pltpu.make_async_remote_copy(
            src_ref=src,
            dst_ref=dst,
            send_sem=ssem,
            recv_sem=rsem,
            device_id=where,
            device_id_type=pl.DeviceIdType.MESH,
        )

    proj_refs = (kw_ref, vw_ref, cvw_ref, cgw_ref, qw_ref, ogw_ref)
    out_refs = (cow_ref, row_ref)

    tok_copy = pltpu.make_async_copy(tok_ref, tok, loc_sem.at[0])
    tok_copy.start()
    barrier = pltpu.get_barrier_semaphore()

    def greet_sp(d, c):
        pl.semaphore_signal(
            barrier,
            inc=1,
            device_id={"sp": lax.rem(me + d, n_s)},
            device_id_type=pl.DeviceIdType.MESH,
        )
        return c

    def greet_tp(d, c):
        pl.semaphore_signal(
            barrier,
            inc=1,
            device_id={"tp": lax.rem(mt + d, n_t)},
            device_id_type=pl.DeviceIdType.MESH,
        )
        return c

    lax.fori_loop(1, n_s, greet_sp, 0)
    lax.fori_loop(1, n_t, greet_tp, 0)

    def wslot(b, m):
        return wbuf.at[m, pl.ds(pl.multiple_of(b * wrows, wrows), wrows)]

    def oslot(s, m):
        return obuf.at[m, pl.ds(pl.multiple_of(s * wrows, wrows), wrows)]

    local = [
        pltpu.make_async_copy(r, wslot(idx, m), loc_sem.at[1 + m]) for m, r in enumerate(proj_refs)
    ] + [
        pltpu.make_async_copy(r, oslot(me, m), loc_sem.at[1 + N_PROJ + m])
        for m, r in enumerate(out_refs)
    ]
    for copy in local:
        copy.start()

    pl.semaphore_wait(barrier, n_s - 1 + n_t - 1)

    has_right = idx + 1 < n_o
    has_left = idx >= 1
    right = member(jnp.minimum(idx + 1, n_o - 1))
    left = member(jnp.maximum(idx - 1, 0))

    def w_copy(direction, b, m, src=None):
        slot = wslot(b, m)
        return remote(
            slot if src is None else src,
            slot,
            ws_sem.at[direction, b, m],
            wr_sem.at[direction, b, m],
            {"sp": right if direction == 0 else left},
        )

    @pl.when(has_right)
    def _():
        for m in range(N_PROJ):
            w_copy(0, idx, m, proj_refs[m]).start()

    @pl.when(has_left)
    def _():
        for m in range(N_PROJ):
            w_copy(1, idx, m, proj_refs[m]).start()

    tok_copy.wait()
    step = 256
    square = jnp.zeros((rows, 1), F32)
    for c in range(0, tok.shape[1], step):
        part = tok[:, c : c + step].astype(F32)
        square = square + jnp.sum(part * part, axis=1, keepdims=True)
    scale = lax.rsqrt(square / tok.shape[1] + EPSILON)
    width = k * wrows
    for j in range(n_s // (2 * k)):
        for side, dst in ((1 - half, x_send), (half, x_self)):
            start = pl.multiple_of((2 * j + side) * width, 128)
            part = tok[:, pl.ds(start, width)].astype(F32)
            dst[:, j * width : (j + 1) * width] = (
                part * scale * gain_ref[:, pl.ds(start, width)]
            ).astype(BF16)
    x_copy = remote(x_send, x_recv, x_sem.at[0], x_sem.at[1], {"sp": pair})
    x_copy.start()

    tot_send[...] = jnp.zeros_like(tot_send)
    r_iota = lax.broadcasted_iota(jnp.int32, (rows, rows), 0)
    c_iota = lax.broadcasted_iota(jnp.int32, (rows, rows), 1)
    for h in range(heads):
        ld = ld_ref[h : h + 1, :]
        ld_col = jnp.sum(jnp.where(r_iota == c_iota, ld, 0.0), axis=1, keepdims=True)
        run_col = jnp.sum(jnp.where(c_iota <= r_iota, ld, 0.0), axis=1, keepdims=True)
        run_row = jnp.sum(jnp.where(r_iota <= c_iota, ld_col, 0.0), axis=0, keepdims=True)
        keep = c_iota <= r_iota
        decay[h] = jnp.where(keep, jnp.exp(jnp.where(keep, run_col - run_row, 0.0)), 0.0)
        run_cols[h] = jnp.broadcast_to(run_col, (rows, HEAD_DIM))
        tot_send[h : h + 1, :] = jnp.broadcast_to(run_col[rows - 1 : rows], (1, HEAD_DIM))

    def tot_copy(to, source):
        return remote(
            tot_send, tot_buf.at[source], ts_sem.at[to], tr_sem.at[source], {"sp": to}
        )

    def start_tot(to, c):
        tot_copy(to, me).start()
        return c

    lax.fori_loop(me + 1, n_s, start_tot, 0)

    def pass_on(d, c):
        for m in range(N_PROJ):

            @pl.when(idx - 1 - d >= 0)
            def _():
                b = jnp.maximum(idx - 1 - d, 0)
                w_copy(0, b, m).wait_recv()

                @pl.when(has_right)
                def _():
                    w_copy(0, b, m).start()

            @pl.when(idx + 1 + d < n_o)
            def _():
                b = jnp.minimum(idx + 1 + d, n_o - 1)
                w_copy(1, b, m).wait_recv()

                @pl.when(has_left)
                def _():
                    w_copy(1, b, m).start()

        return c

    lax.fori_loop(0, max(n_o - 2, 0), pass_on, 0)

    def o_copy(direction, s, m, src=None):
        slot = oslot(s, m)
        b = (s // (2 * k)) * k + lax.rem(s, k)
        return remote(
            slot if src is None else src,
            slot,
            os_sem.at[direction, b, m],
            or_sem.at[direction, b, m],
            {"sp": right if direction == 0 else left},
        )

    def y_copy(b, m, arriving=False):
        s = (b // k) * (2 * k) + (1 - half if arriving else half) * k + lax.rem(b, k)
        slot = oslot(s, m)
        return remote(slot, slot, oy_sem.at[0, b, m], oy_sem.at[1, b, m], {"sp": pair})

    def start_out_own():
        for m in range(2):
            local[N_PROJ + m].wait()
            y_copy(idx, m).start()

        @pl.when(has_right)
        def _():
            for m in range(2):
                o_copy(0, me, m).start()

        @pl.when(has_left)
        def _():
            for m in range(2):
                o_copy(1, me, m).start()

    def pass_out(d, c):
        for m in range(2):

            @pl.when(idx - 1 - d >= 0)
            def _():
                b = jnp.maximum(idx - 1 - d, 0)
                o_copy(0, member(b), m).wait_recv()

                @pl.when(has_right)
                def _():
                    o_copy(0, member(b), m).start()

                y_copy(b, m).start()

            @pl.when(idx + 1 + d < n_o)
            def _():
                b = jnp.minimum(idx + 1 + d, n_o - 1)
                o_copy(1, member(b), m).wait_recv()

                @pl.when(has_left)
                def _():
                    o_copy(1, member(b), m).start()

                y_copy(b, m).start()

        return c

    start_out_own()

    cb, sb = cb_ref[me], sb_ref[me]
    lane = lax.broadcasted_iota(jnp.int32, (rows, HEAD_DIM), 1)
    cos = cj_ref[...] * cb - sj_ref[...] * sb
    sin = sj_ref[...] * cb + cj_ref[...] * sb
    sin = jnp.where(lane < HEAD_DIM // 2, -sin, sin)

    def rotate(x):
        return x * cos + pltpu.roll(x, HEAD_DIM // 2, 1) * sin

    x_copy.wait_recv()

    def p_copy(m):
        return remote(p_send.at[m], p_recv.at[m], p_sem.at[0, m], p_sem.at[1, m], {"sp": pair})

    def last_block(m):
        @pl.when(jnp.logical_and(idx - 1 - (n_o - 2) >= 0, n_o >= 2))
        def _():
            w_copy(0, 0, m).wait_recv()

        @pl.when(jnp.logical_and(idx + 1 + (n_o - 2) < n_o, n_o >= 2))
        def _():
            w_copy(1, n_o - 1, m).wait_recv()

    def multiply(m):
        local[m].wait()
        last_block(m)
        p_send[m] = dot(x_recv[...], wbuf[m]).astype(BF16)
        p_copy(m).start()
        acc[m] = dot(x_self[...], wbuf[m])

    def projected(m):
        p_copy(m).wait_recv()
        return (acc[m] + p_recv[m].astype(F32)).astype(BF16)

    def head(x, h):
        return x[:, h * HEAD_DIM : (h + 1) * HEAD_DIM]

    def st_copy(to, source):
        return remote(st_send, st_buf.at[source], ss_sem.at[to], sr_sem.at[source], {"sp": to})

    multiply(0)
    multiply(1)
    multiply(2)
    key_raw, value = projected(0), projected(1)
    qkv[1] = value
    for h in range(heads):
        at = slice(h * HEAD_DIM, (h + 1) * HEAD_DIM)
        key = rotate(head(key_raw, h).astype(F32)).astype(BF16)
        qkv[0, :, at] = key
        run = run_cols[h]
        weighted = (key.astype(F32) * jnp.exp(run[rows - 1 : rows] - run)).astype(BF16)
        st_send[at, :] = dot(weighted, head(value, h), 0, 0).astype(BF16)

    def start_state(to, c):
        st_copy(to, me).start()
        return c

    lax.fori_loop(me + 1, n_s, start_state, 0)

    multiply(3)
    gated = (
        projected(2).astype(F32) * jax.nn.sigmoid(projected(3).astype(F32))
    ).astype(BF16)
    halo_send[...] = gated[rows - HALO :]
    after = lax.rem(me + 1, n_s)
    h_copy = remote(halo_send, halo_recv, h_sem.at[0], h_sem.at[1], {"sp": after})
    h_copy.start()
    xp[HALO:, :] = gated.astype(F32)
    multiply(4)
    multiply(5)
    third = -(-(n_o - 1) // 3)
    lax.fori_loop(0, min(third, n_o - 1), pass_out, 0)

    h_copy.wait_recv()
    xp[:HALO, :] = jnp.where(me > 0, halo_recv[...].astype(F32), 0.0)
    col0 = pl.multiple_of(mt * cols, 128)
    n_taps = taps_ref.shape[0]
    taps = taps_ref[:, pl.ds(col0, cols)].astype(F32)
    total = jnp.zeros((rows, 1), F32)
    totsq = jnp.zeros((rows, 1), F32)
    for c in range(0, cols, 128):
        for r in range(0, rows, 64):
            s = jnp.zeros((64, 128), F32)
            for w in range(n_taps):
                first = r + w + HALO - (n_taps - 1)
                s = s + xp[first : first + 64, c : c + 128] * taps[w : w + 1, c : c + 128]
            csum[r : r + 64, c : c + 128] = s
    conv = csum[...]
    total = jnp.sum(conv, axis=1, keepdims=True)
    totsq = jnp.sum(conv * conv, axis=1, keepdims=True)
    diag = r_iota == c_iota
    stat_send[...] = jnp.zeros_like(stat_send)
    stat_send[0:1, :rows] = jnp.sum(jnp.where(diag, total, 0.0), axis=0, keepdims=True)
    stat_send[1:2, :rows] = jnp.sum(jnp.where(diag, totsq, 0.0), axis=0, keepdims=True)

    def stat_copy(d):
        to = lax.rem(mt + d, n_t)
        return remote(
            stat_send, stat_buf.at[d - 1], stat_sem.at[0, d - 1], stat_sem.at[1, d - 1], {"tp": to}
        )

    for d in range(1, n_t):
        stat_copy(d).start()

    lax.fori_loop(min(third, n_o - 1), min(2 * third, n_o - 1), pass_out, 0)

    query_raw = projected(4)
    for h in range(heads):
        at = slice(h * HEAD_DIM, (h + 1) * HEAD_DIM)
        query = (rotate(head(query_raw, h).astype(F32)) * HEAD_DIM ** (-0.5)).astype(BF16)
        qkv[2, :, at] = query
        weights = (dot(query, qkv[0, :, at], 1, 1) * decay[h]).astype(BF16)
        csum_h = dot(weights, qkv[1, :, at])
        acc[0, :, at] = csum_h

    state[...] = jnp.zeros_like(state)

    def carry(s, c):
        tot_copy(me, s).wait_recv()
        st_copy(me, s).wait_recv()
        for h in range(heads):
            at = slice(h * HEAD_DIM, (h + 1) * HEAD_DIM)
            factor = jnp.exp(tot_buf[s, h : h + 1, :])
            state[at, :] = state[at, :] * factor + st_buf[s, at, :].astype(F32)
        return c

    lax.fori_loop(0, me, carry, 0)
    out_gate = projected(5).astype(F32)
    gate = out_gate * jax.nn.sigmoid(out_gate)
    for h in range(heads):
        at = slice(h * HEAD_DIM, (h + 1) * HEAD_DIM)
        cross = dot(qkv[2, :, at], state[at, :].astype(BF16)) * jnp.exp(run_cols[h])
        merged = acc[0, :, at] + cross
        mean = jnp.mean(merged, axis=1, keepdims=True)
        away = merged - mean
        var = jnp.mean(away * away, axis=1, keepdims=True)
        rg = rgain_ref[:, pl.ds(pl.multiple_of(mt * cols + h * HEAD_DIM, 128), HEAD_DIM)]
        hid[1, :, at] = (gate[:, at] * (away * lax.rsqrt(var + EPSILON)) * rg).astype(BF16)

    lax.fori_loop(min(2 * third, n_o - 1), n_o - 1, pass_out, 0)

    sums = stat_send[...]
    for d in range(1, n_t):
        stat_copy(d).wait_recv()
        sums = sums + stat_buf[d - 1]
    total = jnp.sum(jnp.where(diag, sums[0:1, :rows], 0.0), axis=1, keepdims=True)
    totsq = jnp.sum(jnp.where(diag, sums[1:2, :rows], 0.0), axis=1, keepdims=True)
    mean = total / conv_dim
    var = totsq / conv_dim - mean * mean
    normed = (csum[...] - mean) * lax.rsqrt(var + EPSILON) * cgain_ref[:, pl.ds(col0, cols)]
    hid[0] = (normed * jax.nn.sigmoid(normed)).astype(BF16)

    def arrived(b, c):
        for m in range(2):
            y_copy(b, m, True).wait_recv()
        return c

    lax.fori_loop(0, n_o, arrived, 0)
    features = r_send.shape[1]
    fc = features // CHUNKS
    share = rows // n_t

    def r_copy(d, j):
        to = lax.rem(mt + d, n_t)
        at = pl.ds(j * fc, fc)
        return remote(
            r_send.at[pl.ds(pl.multiple_of(to * share, 16), share), at],
            r_buf.at[d - 1, :, at],
            rs_sem.at[0, d - 1, j],
            rs_sem.at[1, d - 1, j],
            {"tp": to},
        )

    for j in range(CHUNKS):
        at = slice(j * fc, (j + 1) * fc)
        r_send[:, at] = (
            dot(hid[0], obuf[0, at, :], 1, 1) + dot(hid[1], obuf[1, at, :], 1, 1)
        ).astype(BF16)
        for d in range(1, n_t):
            r_copy(d, j).start()

    for j in range(CHUNKS):
        at = slice(j * fc, (j + 1) * fc)
        mixed = r_send[pl.ds(pl.multiple_of(mt * share, 16), share), at].astype(F32)
        for d in range(1, n_t):
            r_copy(d, j).wait_recv()
            mixed = mixed + r_buf[d - 1, :, at].astype(F32)
        out_ref[:, at] = mixed.astype(BF16)

    x_copy.wait_send()
    h_copy.wait_send()
    for m in range(N_PROJ):
        p_copy(m).wait_send()
    for d in range(1, n_t):
        stat_copy(d).wait_send()
        for j in range(CHUNKS):
            r_copy(d, j).wait_send()

    def sent_later(to, c):
        tot_copy(to, me).wait_send()
        st_copy(to, me).wait_send()
        return c

    lax.fori_loop(me + 1, n_s, sent_later, 0)

    def sent_right(b, c):
        for m in range(N_PROJ):
            w_copy(0, b, m).wait_send()
        for m in range(2):
            o_copy(0, member(b), m).wait_send()
        return c

    def sent_left(b, c):
        for m in range(N_PROJ):
            w_copy(1, b, m).wait_send()
        for m in range(2):
            o_copy(1, member(b), m).wait_send()
        return c

    @pl.when(has_right)
    def _():
        lax.fori_loop(0, idx + 1, sent_right, 0)

    @pl.when(has_left)
    def _():
        lax.fori_loop(idx, n_o, sent_left, 0)

    def sent_pair(b, c):
        for m in range(2):
            y_copy(b, m).wait_send()
        return c

    lax.fori_loop(0, n_o, sent_pair, 0)


def tables(n_s, rows):
    freq = ROPE_BASE ** (-np.arange(0, HEAD_DIM, 2, dtype=np.float64) / HEAD_DIM)
    freq = np.concatenate([freq, freq])
    near = np.arange(rows, dtype=np.float64)[:, None] * freq
    base = (np.arange(n_s, dtype=np.float64) * rows)[:, None, None] * freq
    return [np.float32(f(a)) for a in (near, base) for f in (np.cos, np.sin)]


def solution(mesh):
    n_s, n_t = mesh.shape["sp"], mesh.shape["tp"]

    def per_device(
        tokens,
        norm_gain,
        conv_value_w,
        conv_gate_w,
        query_w,
        key_w,
        value_w,
        out_gate_w,
        conv_out_w,
        ret_out_w,
        conv_taps,
        conv_gain,
        ret_gain,
        log_decay,
    ):
        rows, d = tokens.shape
        wrows, cols = query_w.shape
        n_o = n_s // 2
        heads = cols // HEAD_DIM
        share = rows // n_t
        vmem = pl.BlockSpec(memory_space=pltpu.VMEM)
        hbm = pl.BlockSpec(memory_space=pl.ANY)
        dma = pltpu.SemaphoreType.DMA
        call = pl.pallas_call(
            functools.partial(kernel, n_s, n_t, conv_gain.shape[0]),
            out_shape=jax.ShapeDtypeStruct((share, d), BF16),
            in_specs=[hbm, vmem] + [hbm] * 8 + [vmem] * 8,
            out_specs=vmem,
            scratch_shapes=[
                pltpu.VMEM((rows, d), BF16),
                pltpu.VMEM((rows, d // 2), BF16),
                pltpu.VMEM((rows, d // 2), BF16),
                pltpu.VMEM((rows, d // 2), BF16),
                pltpu.VMEM((N_PROJ, d // 2, cols), BF16),
                pltpu.VMEM((2, d, cols), BF16),
                pltpu.VMEM((N_PROJ, rows, cols), F32),
                pltpu.VMEM((N_PROJ, rows, cols), BF16),
                pltpu.VMEM((N_PROJ, rows, cols), BF16),
                pltpu.VMEM((heads, rows, rows), F32),
                pltpu.VMEM((heads, rows, HEAD_DIM), F32),
                pltpu.VMEM((8, HEAD_DIM), F32),
                pltpu.VMEM((n_s, 8, HEAD_DIM), F32),
                pltpu.VMEM((cols, HEAD_DIM), BF16),
                pltpu.VMEM((n_s, cols, HEAD_DIM), BF16),
                pltpu.VMEM((cols, HEAD_DIM), F32),
                pltpu.VMEM((HALO, cols), BF16),
                pltpu.VMEM((HALO, cols), BF16),
                pltpu.VMEM((HALO + rows, cols), F32),
                pltpu.VMEM((rows, cols), F32),
                pltpu.VMEM((8, 256), F32),
                pltpu.VMEM((n_t - 1, 8, 256), F32),
                pltpu.VMEM((2, rows, cols), BF16),
                pltpu.VMEM((rows, d), BF16),
                pltpu.VMEM((n_t - 1, share, d), BF16),
                pltpu.VMEM((3, rows, cols), BF16),
                dma((1 + N_PROJ + 2,)),
                dma((2,)),
                dma((2, n_o, N_PROJ)),
                dma((2, n_o, N_PROJ)),
                dma((2, n_o, 2)),
                dma((2, n_o, 2)),
                dma((2, n_o, 2)),
                dma((2, N_PROJ)),
                dma((n_s,)),
                dma((n_s,)),
                dma((n_s,)),
                dma((n_s,)),
                dma((2,)),
                dma((2, n_t - 1)),
                dma((2, n_t - 1, CHUNKS)),
            ],
            compiler_params=pltpu.CompilerParams(
                collective_id=0, has_side_effects=True, vmem_limit_bytes=48 * 1024 * 1024
            ),
        )
        cj, sj, cb, sb = tables(n_s, rows)
        return call(
            tokens,
            norm_gain[None, :],
            key_w,
            value_w,
            conv_value_w,
            conv_gate_w,
            query_w,
            out_gate_w,
            conv_out_w,
            ret_out_w,
            conv_taps,
            conv_gain[None, :],
            ret_gain[None, :],
            log_decay,
            cj,
            sj,
            cb,
            sb,
        )

    return jax.shard_map(
        per_device,
        mesh=mesh,
        in_specs=(
            P("sp", None),
            P(),
            P("sp", "tp"),
            P("sp", "tp"),
            P("sp", "tp"),
            P("sp", "tp"),
            P("sp", "tp"),
            P("sp", "tp"),
            P("sp", "tp"),
            P("sp", "tp"),
            P(),
            P(),
            P(),
            P("tp", "sp"),
        ),
        out_specs=P(("sp", "tp"), None),
        check_vma=False,
    )
```

time: 375 us -> 113 us (0.30)
  waiting for transfers between devices: 285 us -> 0 us
  Pallas kernels: 0 us -> 97.1 us
  blocking collectives: 47.6 us -> 0 us
  matrix products: 14.7 us -> 0 us
  between operations: 14.1 us -> 0.03 us
  local copies, waits for them, and re-layouts: 3.54 us -> 15.1 us
  other arithmetic: 4.59 us -> 0 us
    all_gather x8 -> x0, waiting for transfers between devices: 253 us -> none  [the longest x1 41.1 us: per_device(): lax.all_gather(ret_out_w, 'sp', axis=0, tiled=True)]
    pallas_call x0 -> x1, Pallas kernels: none -> 97.1 us  [per_device(): call(tokens, norm_gain[None, :], key_w, value_w, conv_value_w, conv_gate_...]
    reduce_scatter x1 -> x0, waiting for transfers between devices: 25.3 us -> none  [per_device(): lax.psum_scatter((conv_term + ret_term).astype(jnp.bfloat16), 'tp', scatt...]
    all_gather x1 -> x0, blocking collectives: 24.8 us -> none  [carried_in(): lax.all_gather(part.astype(kind), axis)]
    dot_general x10 -> x0, matrix products: 14.7 us -> none  [the longest x5 8.24 us: project(): jnp.dot(normed, weight, preferred_element_type=jnp.float32)]
    unnamed x13 -> x37, local copies, waits for them, and re-layouts: 0.96 us -> 15.1 us
    unnamed x1 -> x0, blocking collectives: 14 us -> none
    psum x1 -> x0, blocking collectives: 8.89 us -> none  [per_device(): lax.psum((jnp.sum(conv_sum, axis=-1), jnp.sum(conv_sum * conv_sum, axis=-...]
  transfers between devices with their start and end apart: 10 -> 0, of which waited for: 10 -> 0; matrix products, arithmetic and copies ran while one was open for 5% -> 0% of each run, Pallas kernels for 0% -> 0%
where the time goes in v1:
time: 113 us; the launch traced here: 112 us
  Pallas kernels  97.1 us (86%)
  local copies, waits for them, and re-layouts  15.1 us (13%)
    pallas_call x1, Pallas kernels, per_device(): call(tokens, norm_gain[None, :], key_w, value_w, conv_value_w, conv_gate_...  97.1 us
    unnamed x37, local copies, waits for them, and re-layouts  15.1 us

profile of v1, /device:TPU:25, one launch (start us, length us, event | category | flops | bytes accessed | tf_op | source)
XLA Modules:
  0.0 112.2 jit_solution(153408537890703621)
XLA Ops:
  0.0 0.0 copy-start.15
  0.0 0.0 copy-start.13
  0.0 0.7 copy-done.15
  0.7 0.0 copy-done.13
  0.7 0.0 copy-start
  0.7 1.1 %copy-done = bf16[192,2048]{1,0:T(8,128)(2,1)S(1)} copy-done((bf16[192,2048]{1,0:T(8,128)(2,1)S(1)}, bf16[192,2048]{1,0:T(8,128)(2,1)}, u32[]{:S(2)}) %copy-start) | copy-done | bytes 786456
  1.8 0.0 copy-start.1
  1.8 0.9 copy-done.1
  2.7 0.0 copy-start.2
  2.7 0.9 copy-done.2
  3.6 0.0 copy-start.3
  3.6 0.9 copy-done.3
  4.6 0.0 copy-start.4
  4.6 0.9 copy-done.4
  5.5 0.0 copy-start.5
  5.5 0.9 copy-done.5
  6.4 0.0 copy-start.6
  6.4 0.9 copy-done.6
  7.3 0.0 copy-start.7
  7.3 0.9 copy-done.7
  8.2 0.0 copy-start.8
  8.2 0.9 copy-done.8
  9.1 0.0 copy-start.9
  9.1 0.9 copy-done.9
  10.0 0.0 copy-start.10
  10.0 0.9 copy-done.10
  10.9 0.0 copy-start.11
  10.9 0.8 copy-done.11
  11.7 0.0 copy-start.12
  11.7 0.7 copy-done.12
  12.4 0.0 copy-start.14
  12.4 0.7 copy-done.14
  13.1 0.0 copy-start.16
  13.1 0.7 copy-done.16
  13.8 0.0 copy-start.17
  13.8 0.7 copy-done.17
  14.5 97.1 %shard_map.172 = bf16[48,2048]{1,0:T(8,128)(2,1)S(1)} custom-call(bf16[192,2048]{1,0:T(8,128)(2,1)S(1)} %copy-done, f32[1,2048]{1,0:T(1,128)S(1)} %bitcast.3, bf16[256,256]{1,0:T(8,128)(2,1)S(1)} %copy-done.1, bf16[256,256]{1,0:T(8,128)(2,1)S(1)} %copy-done.2, bf16[256,256]{1,0:T(8,128)(2,1)S(1)} %copy-done.3, bf16[256,256]{1,0:T(8,128)(2,1)S(1)} %copy-done.4, ...), custom_call_target="tpu_custom_call" | custom-call | tf_op jit(solution)/shard_map/pallas_call | solution.py:634
  111.6 0.7 copy.20
Async XLA Ops:
  0.0 0.7 copy-start.15
  0.0 0.7 copy-start.13
  0.7 1.1 %copy-start = (bf16[192,2048]{1,0:T(8,128)(2,1)S(1)}, bf16[192,2048]{1,0:T(8,128)(2,1)}, u32[]{:S(2)}) copy-start(bf16[192,2048]{1,0:T(8,128)(2,1)} %tok_ref.1) | copy-start | bytes 2359300
  1.8 0.9 copy-start.1
  2.7 0.9 copy-start.2
  3.6 0.9 copy-start.3
  4.6 0.9 copy-start.4
  5.5 0.9 copy-start.5
  6.4 0.9 copy-start.6
  7.3 0.9 copy-start.7
  8.2 0.9 copy-start.8
  9.1 0.9 copy-start.9
  10.0 0.9 copy-start.10
  10.9 0.8 copy-start.11
  11.7 0.7 copy-start.12
  12.4 0.7 copy-start.14
  13.1 0.7 copy-start.16
  13.8 0.7 copy-start.17

commit v2 on v1

--- a/solution.py
+++ b/solution.py
@@ -27,7 +27,7 @@
     n_t,
     conv_dim,
     tok_ref,
-    gain_ref,
+    gain_hbm,
     kw_ref,
     vw_ref,
     cvw_ref,
@@ -36,16 +36,24 @@
     ogw_ref,
     cow_ref,
     row_ref,
+    taps_hbm,
+    cgain_hbm,
+    rgain_hbm,
+    ld_hbm,
+    near_hbm,
+    base_hbm,
+    out_ref,
+    tok,
+    gain_ref,
     taps_ref,
     cgain_ref,
     rgain_ref,
     ld_ref,
-    cj_ref,
-    sj_ref,
-    cb_ref,
-    sb_ref,
-    out_ref,
-    tok,
+    near,
+    base,
+    x_end,
+    ret_own,
+    ret_send,
     x_self,
     x_send,
     x_recv,
@@ -86,6 +94,9 @@
     h_sem,
     stat_sem,
     rs_sem,
+    small_sem,
+    e_sem,
+    q_sem,
 ):
     rows = tok.shape[0]
     wrows, cols = kw_ref.shape
@@ -151,7 +162,22 @@
         pltpu.make_async_copy(r, oslot(me, m), loc_sem.at[1 + N_PROJ + m])
         for m, r in enumerate(out_refs)
     ]
-    for copy in local:
+    col0 = pl.multiple_of(mt * cols, 128)
+    small = [
+        pltpu.make_async_copy(src, dst, small_sem.at[n])
+        for n, (src, dst) in enumerate(
+            (
+                (gain_hbm, gain_ref),
+                (ld_hbm, ld_ref),
+                (taps_hbm.at[:, pl.ds(col0, cols)], taps_ref),
+                (cgain_hbm.at[:, pl.ds(col0, cols)], cgain_ref),
+                (rgain_hbm.at[:, pl.ds(col0, cols)], rgain_ref),
+                (near_hbm, near),
+                (base_hbm.at[me], base),
+            )
+        )
+    ]
+    for copy in small + local:
         copy.start()
 
     pl.semaphore_wait(barrier, n_s - 1 + n_t - 1)
@@ -182,6 +208,8 @@
             w_copy(1, idx, m, proj_refs[m]).start()
 
     tok_copy.wait()
+    for copy in small:
+        copy.wait()
     step = 256
     square = jnp.zeros((rows, 1), F32)
     for c in range(0, tok.shape[1], step):
@@ -308,10 +336,10 @@
 
     start_out_own()
 
-    cb, sb = cb_ref[me], sb_ref[me]
+    cb, sb = base[0:1, :], base[1:2, :]
     lane = lax.broadcasted_iota(jnp.int32, (rows, HEAD_DIM), 1)
-    cos = cj_ref[...] * cb - sj_ref[...] * sb
-    sin = sj_ref[...] * cb + cj_ref[...] * sb
+    cos = near[0] * cb - near[1] * sb
+    sin = near[1] * cb + near[0] * sb
     sin = jnp.where(lane < HEAD_DIM // 2, -sin, sin)
 
     def rotate(x):
@@ -383,11 +411,8 @@
 
     h_copy.wait_recv()
     xp[:HALO, :] = jnp.where(me > 0, halo_recv[...].astype(F32), 0.0)
-    col0 = pl.multiple_of(mt * cols, 128)
     n_taps = taps_ref.shape[0]
-    taps = taps_ref[:, pl.ds(col0, cols)].astype(F32)
-    total = jnp.zeros((rows, 1), F32)
-    totsq = jnp.zeros((rows, 1), F32)
+    taps = taps_ref[...].astype(F32)
     for c in range(0, cols, 128):
         for r in range(0, rows, 64):
             s = jnp.zeros((64, 128), F32)
@@ -444,7 +469,7 @@
         mean = jnp.mean(merged, axis=1, keepdims=True)
         away = merged - mean
         var = jnp.mean(away * away, axis=1, keepdims=True)
-        rg = rgain_ref[:, pl.ds(pl.multiple_of(mt * cols + h * HEAD_DIM, 128), HEAD_DIM)]
+        rg = rgain_ref[:, at]
         hid[1, :, at] = (gate[:, at] * (away * lax.rsqrt(var + EPSILON)) * rg).astype(BF16)
 
     lax.fori_loop(min(2 * third, n_o - 1), n_o - 1, pass_out, 0)
@@ -457,7 +482,7 @@
     totsq = jnp.sum(jnp.where(diag, sums[1:2, :rows], 0.0), axis=1, keepdims=True)
     mean = total / conv_dim
     var = totsq / conv_dim - mean * mean
-    normed = (csum[...] - mean) * lax.rsqrt(var + EPSILON) * cgain_ref[:, pl.ds(col0, cols)]
+    normed = (csum[...] - mean) * lax.rsqrt(var + EPSILON) * cgain_ref[...]
     hid[0] = (normed * jax.nn.sigmoid(normed)).astype(BF16)
 
     def arrived(b, c):
@@ -548,7 +573,9 @@
     freq = np.concatenate([freq, freq])
     near = np.arange(rows, dtype=np.float64)[:, None] * freq
     base = (np.arange(n_s, dtype=np.float64) * rows)[:, None, None] * freq
-    return [np.float32(f(a)) for a in (near, base) for f in (np.cos, np.sin)]
+    near = np.stack([np.cos(near), np.sin(near)])
+    base = np.concatenate([np.cos(base), np.sin(base), np.zeros((n_s, 6, HEAD_DIM))], axis=1)
+    return np.float32(near), np.float32(base)
 
 
 def solution(mesh):
@@ -581,10 +608,20 @@
         call = pl.pallas_call(
             functools.partial(kernel, n_s, n_t, conv_gain.shape[0]),
             out_shape=jax.ShapeDtypeStruct((share, d), BF16),
-            in_specs=[hbm, vmem] + [hbm] * 8 + [vmem] * 8,
+            in_specs=[hbm] * 16,
             out_specs=vmem,
             scratch_shapes=[
                 pltpu.VMEM((rows, d), BF16),
+                pltpu.VMEM((1, d), F32),
+                pltpu.VMEM((conv_taps.shape[0], cols), BF16),
+                pltpu.VMEM((1, cols), F32),
+                pltpu.VMEM((1, cols), F32),
+                pltpu.VMEM(log_decay.shape, F32),
+                pltpu.VMEM((2, rows, HEAD_DIM), F32),
+                pltpu.VMEM((8, HEAD_DIM), F32),
+                pltpu.VMEM((2, rows, d // 2), BF16),
+                pltpu.VMEM((N_PROJ, rows, cols), BF16),
+                pltpu.VMEM((2, N_PROJ, rows, cols), BF16),
                 pltpu.VMEM((rows, d // 2), BF16),
                 pltpu.VMEM((rows, d // 2), BF16),
                 pltpu.VMEM((rows, d // 2), BF16),
@@ -625,12 +662,15 @@
                 dma((2,)),
                 dma((2, n_t - 1)),
                 dma((2, n_t - 1, CHUNKS)),
+                dma((7,)),
+                dma((2, 2)),
+                dma((2, 2, N_PROJ)),
             ],
             compiler_params=pltpu.CompilerParams(
-                collective_id=0, has_side_effects=True, vmem_limit_bytes=48 * 1024 * 1024
+                collective_id=0, has_side_effects=True, vmem_limit_bytes=67043328
             ),
         )
-        cj, sj, cb, sb = tables(n_s, rows)
+        near, base = tables(n_s, rows)
         return call(
             tokens,
             norm_gain[None, :],
@@ -646,10 +686,8 @@
             conv_gain[None, :],
             ret_gain[None, :],
             log_decay,
-            cj,
-            sj,
-            cb,
-            sb,
+            near,
+            base,
         )
 
     return jax.shard_map(

time: 113 us -> 99.6 us (0.88)
  local copies, waits for them, and re-layouts: 15.1 us -> 1.62 us
    unnamed x37 -> x1, local copies, waits for them, and re-layouts: 15.1 us -> 1.62 us
where the time goes in v2:
time: 99.6 us; the launch traced here: 99.5 us
  Pallas kernels  97.8 us (98%)
  local copies, waits for them, and re-layouts  1.62 us (2%)
    pallas_call x1, Pallas kernels, per_device(): call(tokens, norm_gain[None, :], key_w, value_w, conv_value_w, conv_gate_...  97.8 us

profile of v2, /device:TPU:25, one launch (start us, length us, event | category | flops | bytes accessed | tf_op | source)
XLA Modules:
  0.0 99.5 jit_solution(8810344336320507552)
XLA Ops:
  0.0 97.8 %shard_map.154 = bf16[48,2048]{1,0:T(8,128)(2,1)} custom-call(bf16[192,2048]{1,0:T(8,128)(2,1)} %tok_ref.1, f32[1,2048]{1,0:T(1,128)} %bitcast.3, bf16[256,256]{1,0:T(8,128)(2,1)} %kw_ref.1, bf16[256,256]{1,0:T(8,128)(2,1)} %vw_ref.1, bf16[256,256]{1,0:T(8,128)(2,1)} %cvw_ref.1, bf16[256,256]{1,0:T(8,128)(2,1)} %cgw_ref.1, bf16[256,256]{1,0:T(8,128)(2,1)} %qw_ref.1, ...), custom_call_target="tpu_custom_call" | custom-call | tf_op jit(solution)/shard_map/pallas_call | solution.py:674
  97.9 1.6 %copy.18 = bf16[48,2048]{1,0:T(8,128)(2,1)} copy(bf16[48,2048]{1,0:T(8,128)(2,1)} %shard_map.154) | data formatting | bytes 393216
